TPU v7x, 32 devices: a whole 2x2x4 slice. The times are simulated.
32 devices in a mesh: sp: 8 (over z, x), tp: 4 (over y, core).
Axes of the slice: x: 2, y: 2, z: 4, core: 2. Of those that a mesh axis runs over, the one named last changes fastest.
Arguments:
- stream_in: bfloat16 [2048, 2048], P(('sp', 'tp')), may hold values from -6 to 6
- queries: bfloat16 [2048, 4096], P('sp', 'tp'), may hold values from -6 to 6
- key_rows: bfloat16 [2048, 4096], P('sp', 'tp'), may hold values from -6 to 6
- values: bfloat16 [2048, 8192], P('sp', 'tp'), may hold values from -6 to 6
- decay_low: bfloat16 [2048, 16], P('sp'), may hold values from -4 to 4
- decay_matrix: bfloat16 [16, 4096], P(None, 'tp'), may hold values from -1.5 to 1.5
- decay_bias: float32 [4096], P('tp')
- decay_shift: float32 [2048, 16], P('sp', 'tp'), may hold values from -1 to 0
- head_gain: float32 [512], replicated, may hold values from 0.1 to 1.9
- output_matrix: bfloat16 [8192, 2048], P('tp'), may hold values from -0.0625 to 0.0625
- feed_gain: float32 [2048], replicated, may hold values from 0.1 to 1.9
- routes: int32 [2048, 2], P('sp'), may hold values from 0 to 7, all different within a row; in each aligned block of 256 rows (0 to 255, 256 to 511, ...) at most 64 rows name the same one
- route_weights: float32 [2048, 2], P('sp'), may hold values from 0.2 to 1
- expert_gate: bfloat16 [8, 2048, 2816], P('sp', None, 'tp'), may hold values from -0.125 to 0.125
- specialist_widen: bfloat16 [8, 2048, 2816], P('sp', None, 'tp'), may hold values from -0.125 to 0.125
- expert_down: bfloat16 [8, 2816, 2048], P('sp', 'tp'), may hold values from -0.109375 to 0.109375
Outputs:
- layer_out: bfloat16 [2048, 2048], P(('sp', 'tp'))
Inputs may be any that keep to these rules, and one draw needn't show every extreme that they name: `routes`: each row names 2 different experts; within each aligned block of 256 rows no expert is named by more than 64 rows, and in every draw some expert is named by exactly 64 rows of some block.
All inputs are finite; a program needn't handle non-finite values.
Results may differ from a plain program's by a relative error of at most 0.02.
Values may be sent and summed in bfloat16 or wider, within the bound.
A program may use at most 128 MiB of HBM per device.

v0:
```python
import jax
import jax.numpy as jnp
from jax import lax
from jax.sharding import PartitionSpec as P

HK = 256
HV = 512
TOP = 2
BLK = 128


TEMPER = 16.0
EPSILON = 1e-06
HIGHEST = lax.Precision.HIGHEST


def entering(shard, axis, combine, identity):
    peers, here = (lax.axis_size(axis), lax.axis_index(axis))
    everything = jax.tree.map(
        lambda part, kind: lax.all_gather(part.astype(kind), axis),
        shard,
        (jnp.bfloat16, jnp.bfloat16),
    )
    start = jax.tree.map(
        lambda part, zero: jnp.broadcast_to(jnp.asarray(zero, part.dtype), part.shape),
        shard,
        identity,
    )

    def step(k, before):
        reached = k < here
        new = combine(
            before, jax.tree.map(lambda part, own: part[k].astype(own.dtype), everything, shard)
        )
        return jax.tree.map(lambda a, b: jnp.where(reached, a, b), new, before)

    return lax.fori_loop(0, peers, step, start)


def decay_logs(decay_low, decay_matrix, decay_bias, decay_shift, heads):
    before_gate = jnp.dot(decay_low, decay_matrix, preferred_element_type=jnp.float32) + decay_bias
    logged = jax.nn.log_sigmoid(before_gate) / TEMPER
    return logged.reshape(before_gate.shape[0], heads, HK) + decay_shift[:, :, None]


def into_blocks(array):
    length, heads, width = array.shape
    return array.reshape(length // BLK, BLK, heads, width).transpose(2, 0, 1, 3)


def segment_summands(queries, key_rows, values, log_decay):
    inside = jnp.cumsum(log_decay, axis=2)
    final_position = inside[:, :, -1:, :]
    scaled_query = queries * jnp.exp(inside) * HK ** (-0.5)
    scaled_key = key_rows * jnp.exp(-inside)
    end_keys = key_rows * jnp.exp(final_position - inside)
    scores = jnp.einsum("hnid,hnjd->hnij", scaled_query, scaled_key, precision=HIGHEST)
    causal = jnp.tril(jnp.ones((BLK, BLK), jnp.bool_))
    scores = jnp.where(causal, scores, 0.0)
    local_out = jnp.einsum("hnij,hnjv->hniv", scores, values, precision=HIGHEST)
    partial_update = jnp.einsum("hnjd,hnjv->hndv", end_keys, values, precision=HIGHEST)
    return (scaled_query, local_out, partial_update, jnp.exp(final_position[:, :, 0, :]))


def run_blocks(scaled_query, partial_update, block_decay, start):

    def advance(state, pieces):
        query_block, added, decay = pieces
        output = jnp.einsum("hid,hdv->hiv", query_block, state, precision=HIGHEST)
        return (state * decay[:, :, None] + added, output)

    final, outputs = lax.scan(
        advance,
        start,
        (
            jnp.moveaxis(scaled_query, 1, 0),
            jnp.moveaxis(partial_update, 1, 0),
            jnp.moveaxis(block_decay, 1, 0),
        ),
    )
    return (final, jnp.moveaxis(outputs, 0, 1))


def link_states(earlier, later):
    return (earlier[0] * later[0], earlier[1] * later[0][..., None] + later[1])


def pass_state(device_decay, local_state):
    identity = (jnp.ones_like(device_decay), jnp.zeros_like(local_state))
    _, carried = entering((device_decay, local_state), "sp", link_states, identity)
    return carried


def head_norm(heads_out, head_gain):
    heads = heads_out.shape[0]
    flat = heads_out.transpose(1, 2, 0, 3).reshape(-1, heads, HV)
    normed = flat * lax.rsqrt(jnp.mean(flat * flat, axis=-1, keepdims=True) + EPSILON) * head_gain
    return normed.reshape(-1, heads * HV).astype(jnp.bfloat16)


def root_scale(midstream, gain):
    return (
        midstream
        * lax.rsqrt(jnp.mean(midstream * midstream, axis=-1, keepdims=True) + EPSILON)
        * gain
    ).astype(jnp.bfloat16)


def body(
    stream_in,
    queries,
    key_rows,
    values,
    decay_low,
    decay_matrix,
    decay_bias,
    decay_shift,
    head_gain,
    output_matrix,
    feed_gain,
    routes,
    route_weights,
    expert_gate,
    specialist_widen,
    expert_down,
):
    length = queries.shape[0]
    heads = queries.shape[1] // HK
    sequence_devices = lax.axis_size("sp")
    head_devices = lax.axis_size("tp")
    width = stream_in.shape[1]
    log_decay = decay_logs(decay_low, decay_matrix, decay_bias, decay_shift, heads)

    def shaped(array, channels):
        return into_blocks(array.astype(jnp.float32).reshape(length, heads, channels))

    scaled_query, local_out, partial_update, block_decay = segment_summands(
        shaped(queries, HK), shaped(key_rows, HK), shaped(values, HV), into_blocks(log_decay)
    )
    start = jnp.zeros((heads, HK, HV), jnp.float32)
    device_decay = jnp.prod(block_decay, axis=1)
    local_state, carried_out = run_blocks(scaled_query, partial_update, block_decay, start)
    carried = pass_state(device_decay, local_state)
    shifted = jnp.concatenate([jnp.ones_like(block_decay[:, :1]), block_decay[:, :-1]], axis=1)
    before = jnp.cumprod(shifted, axis=1)
    readout = jnp.einsum(
        "hnid,hdv->hniv", scaled_query * before[:, :, None, :], carried, precision=HIGHEST
    )
    total_out = local_out + carried_out + readout
    mixed = head_norm(total_out, head_gain)
    rows_here = length // head_devices
    attended = lax.psum_scatter(
        jnp.dot(mixed, output_matrix, preferred_element_type=jnp.float32).astype(jnp.bfloat16),
        "tp",
        scatter_dimension=0,
        tiled=True,
    ).astype(jnp.float32)
    midstream = stream_in.astype(jnp.float32) + attended
    normed = root_scale(midstream, feed_gain)
    group = lax.all_gather(normed, "tp", axis=0, tiled=True)
    experts = sequence_devices * expert_gate.shape[0]
    capacity = head_devices * max(1, TOP * length // (sequence_devices * head_devices))
    block_slots = capacity // head_devices
    own_index = lax.axis_index("tp")
    first_slot = own_index * block_slots
    flat_routes = routes.reshape(-1)
    expert_index = jnp.arange(experts, dtype=jnp.int32)
    matches = (flat_routes[:, None] == expert_index[None, :]).astype(jnp.int32)
    ranking = jnp.sum((jnp.cumsum(matches, axis=0) - matches) * matches, axis=1)

    def slot_table(slot_count, offset):
        slot_member = (
            ranking[:, None] - offset == jnp.arange(slot_count, dtype=jnp.int32)[None, :]
        ).astype(jnp.float32)
        table = slot_member[:, :, None] * matches[:, None, :].astype(jnp.float32)
        return table.reshape(length, TOP, slot_count * experts)

    full_table = slot_table(capacity, 0)
    selector = jnp.sum(slot_table(block_slots, first_slot), axis=1).T.astype(jnp.bfloat16)
    filled = jnp.dot(selector, group, preferred_element_type=jnp.float32)
    shared = lax.all_to_all(
        filled.astype(jnp.bfloat16).reshape(block_slots, experts, width),
        "sp",
        split_axis=1,
        concat_axis=1,
        tiled=True,
    )
    arrived = lax.all_gather(shared, "tp", axis=0, tiled=True)
    rows_in = arrived.reshape(-1, width)
    gated = jnp.dot(rows_in, expert_gate[0], preferred_element_type=jnp.float32)
    lifted = jnp.dot(rows_in, specialist_widen[0], preferred_element_type=jnp.float32)
    hidden = (jax.nn.silu(gated) * lifted).astype(jnp.bfloat16)
    summed = lax.psum_scatter(
        jnp.dot(hidden, expert_down[0], preferred_element_type=jnp.float32).astype(jnp.bfloat16),
        "tp",
        scatter_dimension=0,
        tiled=True,
    )
    expert_token_rows = summed.reshape(block_slots, sequence_devices, width)
    returned = lax.all_to_all(expert_token_rows, "sp", split_axis=1, concat_axis=1, tiled=True)
    weight_table = jnp.sum(full_table * route_weights.reshape(length, TOP, 1), axis=1)
    own_weights = lax.dynamic_slice_in_dim(weight_table, own_index * rows_here, rows_here, 0)
    piece = lax.all_gather(returned, "tp", axis=0, tiled=True)
    count = piece.shape[0]
    flat_piece = piece.reshape(count * experts, width).astype(jnp.float32)
    routed = jnp.dot(own_weights, flat_piece, precision=HIGHEST, preferred_element_type=jnp.float32)
    return (midstream + routed).astype(jnp.bfloat16)


def solution(mesh):
    return jax.shard_map(
        body,
        mesh=mesh,
        in_specs=(
            P(("sp", "tp"), None),
            P("sp", "tp"),
            P("sp", "tp"),
            P("sp", "tp"),
            P("sp", None),
            P(None, "tp"),
            P("tp"),
            P("sp", "tp"),
            P(),
            P("tp", None),
            P(),
            P("sp", None),
            P("sp", None),
            P("sp", None, "tp"),
            P("sp", None, "tp"),
            P("sp", "tp", None),
        ),
        out_specs=P(("sp", "tp"), None),
        check_vma=False,
    )
```

profile of v0, /device:TPU:0, one launch (start us, length us, event | category | flops | bytes accessed | tf_op | source)
XLA Modules:
  0.0 413.3 jit_solution(16421864383166471463)
XLA Ops:
  6.5 2.8 fusion.39
  9.3 2.7 reshape.175
  12.0 2.5 fusion.43
  14.6 4.4 %reduce_window_sum.26 = f32[4,2,128,256]{3,2,1,0:T(8,128)} reduce-window(f32[4,2,128,256]{3,2,1,0:T(8,128)} %fusion.43, f32[]{:T(128)} %constant.77.clone.1), window={size=1x1x128x1 pad=0_0x0_0x127_0x0_0}, to_apply=%region_0.1 | reduce-window | flops 33292288 | bytes 2097156 | tf_op jit(solution)/shard_map/jit(cumsum)/reduce_window_sum | solution.py:52
  18.9 0.8 slice.16
  19.9 1.5 reshape.185
  21.3 2.7 reshape_reshape.16
  24.0 1.4 reshape.184
  25.5 2.8 fusion.40
  28.3 5.8 %convolution_bitcast_fusion = f32[2,4,256,512]{3,2,0,1:T(8,128)} fusion(f32[4,2,128,256]{3,2,1,0:T(8,128)} %reduce_window_sum.26, f32[2,128,4,256]{3,2,1,0:T(4,128)} %reshape.185, bf16[2,128,4,512]{3,2,1,0:T(4,128)(2,1)} %reshape_reshape.16, f32[4,2,256]{2,1,0:T(2,128)S(1)} %bitcast.155), kind=kOutput, calls=%fused_computation.29 | convolution fusion | flops 1611137024 | bytes 7348224 | tf_op jit(solution)/shard_map/hnjd,hnjv->hndv/dot_general | solution.py:61
  34.0 14.5 %while.27 = (s32[]{:T(128)}, f32[4,256,512]{2,1,0:T(8,128)}, f32[2,4,128,512]{3,2,0,1:T(8,128)}, f32[2,4,256]{2,0,1:T(2,128)S(1)}, f32[2,4,256,512]{3,2,0,1:T(8,...) while((s32[]{:T(128)}, f32[4,256,512]{2,1,0:T(8,128)}, f32[2,4,128,512]{3,2,0,1:T(8,128)}, ...), condition=%wide.region_2.3_spmd.clone, body=%wide.region_1.2_spmd.clone.sunk | while | flops 807403520 | bytes 9983080 | solution.py:72
  34.0 3.4 fusion.88
  37.4 3.2 bitcast_add_fusion.4
  40.6 4.1 fusion.88
  44.7 3.8 bitcast_add_fusion.4
  48.6 2.7 convert_element_type.112
  51.5 28.9 %all-gather.2 = bf16[8,4,256]{2,1,0:T(4,128)(2,1)S(1)} all-gather(bf16[1,4,256]{2,1,0:T(4,128)(2,1)S(1)} %bitcast.157), channel_id=2, replica_groups=mesh['sp'=8,'tp'=4] {'sp'}, dimensions={0}, use_global_device_ids=true | all-gather | bytes 18432 | tf_op jit(solution)/shard_map/all_gather | solution.py:20
  80.4 3.8 convolution_select_fusion
  84.2 94.6 %all-gather.14.cloned.1.call-done = bf16[32,256,512]{2,1,0:T(8,128)(2,1)} async-done(((bf16[4,256,512]{2,1,0:T(8,128)(2,1)}), bf16[32,256,512]{2,1,0:T(8,128)(2,1)}) %all-gather.14.cloned.1.call-update) | async-done | bytes 8388624 | tf_op jit(solution)/shard_map/all_gather | solution.py:20
  178.8 27.7 %while.28 = (s32[]{:T(128)}, f32[4,256,512]{2,1,0:T(8,128)}, s32[]{:T(128)}, bf16[8,4,256]{2,1,0:T(4,128)(2,1)S(1)}, bf16[8,4,256,512]{3,2,1,0:T(8,128)(2,1)}, /*index=5*/s32[]{:T(128)}, s32[]{:T(128)}) while((s32[]{:T(128)}, f32[4,256,512]{2,1,0:T(8,128)}, s32[]{:T(128)}, bf16[8,4,256]{2,1,0:T(4,128)(2,1)S(1)}, ...), condition=%wide.region_6.7_spmd.clone, body=%wide.region_5.6_spmd.clone.sunk | while | flops 2622468 | bytes 5253225 | solution.py:37
  178.8 2.9 fusion.89
  181.7 3.5 fusion.89
  185.3 3.5 fusion.89
  188.8 3.5 fusion.89
  192.4 3.5 fusion.89
  195.9 3.5 fusion.89
  199.5 3.5 fusion.89
  203.0 3.5 fusion.89
  206.6 4.5 %fusion.22 = f32[4,2,128,512]{3,2,1,0:T(8,128)S(1)} fusion(f32[4,256,512]{2,1,0:T(8,128)} %get-tuple-element.134, f32[2,128,4,256]{3,2,1,0:T(4,128)} %reshape.184, f32[4,2,128,256]{3,2,1,0:T(8,128)} %reduce_window_sum.26, f32[4,2,256]{2,1,0:T(2,128)S(1)} %broadcast_multiply_fusion.2), kind=kOutput, calls=%fused_computation.30 | convolution fusion | flops 1611137024 | bytes 6299648 | tf_op jit(solution)/shard_map/hnid,hdv->hniv/dot_general | solution.py:146
  211.1 2.8 multiply_reduce_fusion
  213.9 0.1 copy.64
  214.1 0.3 mul.187
  214.4 0.9 copy.77
  215.3 0.7 copy-done.2
  216.0 1.4 copy.51
  217.3 0.9 copy.76
  218.3 6.8 %convolution_convert_fusion.1 = bf16[256,2048]{1,0:T(8,128)(2,1)} fusion(bf16[2048,2048]{1,0:T(8,128)(2,1)} %param.29, f32[256,2048]{1,0:T(8,128)S(1)} %bitcast.151, f32[256,2048]{1,0:T(8,128)S(1)} %bitcast.150, f32[2048]{0:T(1024)S(1)} %bitcast.156), kind=kOutput, calls=%fused_computation.24 | convolution fusion | flops 2149580800 | bytes 13639680 | tf_op jit(solution)/shard_map/dot_general | solution.py:153
  225.1 23.1 %reduce-scatter.3.cloned.1.call-done = bf16[64,2048]{1,0:T(8,128)(2,1)} async-done(((bf16[256,2048]{1,0:T(8,128)(2,1)}), bf16[64,2048]{1,0:T(8,128)(2,1)}) %reduce-scatter.3.cloned.1.call-update) | async-done | bytes 262160 | tf_op jit(solution)/shard_map/reduce_scatter | solution.py:152
  248.2 1.1 multiply_reduce_fusion.2
  249.3 1.8 multiply_convert_fusion.2
  251.1 0.3 all-gather.10.cloned.1.call-start
  251.5 0.1 eq.67
  251.7 0.1 eq.63
  251.8 1.1 reduce-window.9
  253.0 0.2 slice_reduce_fusion
  253.6 4.1 broadcast_multiply_fusion.1
  257.7 4.6 %mul.206 = f32[256,2,128]{2,1,0:T(2,128)} reshape(f32[512,16,8]{2,1,0:T(8,128)} %broadcast_multiply_fusion.1) | data formatting | bytes 524288 | tf_op jit(solution)/shard_map/mul | solution.py:175
  262.3 1.3 reduce_sum.48
  263.6 4.4 %all-gather.8.cloned.1.call-done = bf16[256,2048]{1,0:T(8,128)(2,1)} async-done(((bf16[64,2048]{1,0:T(8,128)(2,1)}), bf16[256,2048]{1,0:T(8,128)(2,1)}) %all-gather.8.cloned.1.call-update) | async-done | bytes 1048592 | tf_op jit(solution)/shard_map/all_gather | solution.py:160
  268.0 1.6 fusion.20
  269.5 0.3 copy.58
  269.8 20.2 %all_to_all.10 = bf16[16,8,2048]{2,0,1:T(8,128)(2,1)S(1)} all-to-all(bf16[16,8,2048]{2,0,1:T(8,128)(2,1)S(1)} %copy.58), channel_id=1, replica_groups=mesh['sp'=8,'tp'=4] {'sp'}, dimensions={1} | all-to-all | bytes 1048576 | tf_op jit(solution)/shard_map/all_to_all | solution.py:181
  290.0 1.1 copy.59
  291.2 20.8 %all-gather.10.cloned.1.call-done = bf16[64,8,2048]{2,1,0:T(8,128)(2,1)} async-done(((bf16[16,8,2048]{2,1,0:T(8,128)(2,1)}), bf16[64,8,2048]{2,1,0:T(8,128)(2,1)}) %all-gather.10.cloned.1.call-update) | async-done | bytes 2097168 | tf_op jit(solution)/shard_map/all_gather | solution.py:188
  312.0 5.2 %fusion.18 = f32[512,704]{0,1:T(8,128)} fusion(bf16[1,2048,704]{1,2,0:T(8,128)(2,1)} %param.33, bf16[64,8,2048]{2,1,0:T(8,128)(2,1)} %all-gather.10.cloned.1.call-done), kind=kOutput, calls=%fused_computation.22 | convolution fusion | flops 1476395008 | bytes 6422528 | tf_op jit(solution)/shard_map/dot_general | solution.py:190
  317.2 7.6 %convolution_convert_fusion = bf16[512,2048]{1,0:T(8,128)(2,1)} fusion(bf16[1,704,2048]{2,1,0:T(8,128)(2,1)S(1)} %copy-done, bf16[1,2048,704]{1,2,0:T(8,128)(2,1)} %param.34, bf16[64,8,2048]{2,1,0:T(8,128)(2,1)} %all-gather.10.cloned.1.call-done, f32[512,704]{0,1:T(8,128)} %fusion.18), kind=kOutput, calls=%fused_computation.18 | convolution fusion | flops 2956001280 | bytes 11403264 | tf_op jit(solution)/shard_map/dot_general | solution.py:194
  324.9 31.3 %reduce-scatter.5.cloned.1.call-done = bf16[128,2048]{1,0:T(8,128)(2,1)} async-done(((bf16[512,2048]{1,0:T(8,128)(2,1)}), bf16[128,2048]{1,0:T(8,128)(2,1)}) %reduce-scatter.5.cloned.1.call-update) | async-done | bytes 524304 | tf_op jit(solution)/shard_map/reduce_scatter | solution.py:193
  356.2 1.3 copy.60
  357.5 19.7 %all_to_all.11 = bf16[16,8,2048]{2,0,1:T(8,128)(2,1)S(1)} all-to-all(bf16[16,8,2048]{2,0,1:T(8,128)(2,1)S(1)} %copy.60), channel_id=1, replica_groups=mesh['sp'=8,'tp'=4] {'sp'}, dimensions={1} | all-to-all | bytes 1048576 | tf_op jit(solution)/shard_map/all_to_all | solution.py:200
  377.2 1.1 copy.61
  378.4 7.7 %broadcast_multiply_fusion = f32[512,64,8]{2,1,0:T(8,128)} fusion(f32[512,8]{1,0:T(8,128)S(1)} %copy.55, f32[512,64]{1,0:T(8,128)S(1)} %fusion.63), kind=kLoop, calls=%fused_computation.16 | loop fusion | flops 262144 | bytes 1196032 | tf_op jit(solution)/shard_map/mul | solution.py:175
  386.1 13.2 %mul.198 = f32[256,2,512]{2,1,0:T(2,128)} reshape(f32[512,64,8]{2,1,0:T(8,128)} %broadcast_multiply_fusion) | data formatting | bytes 2097152 | tf_op jit(solution)/shard_map/mul | solution.py:175
  399.5 3.4 multiply_reduce_fusion.1
  402.8 3.6 fusion.21
  (74 shorter events, 1.3 us)
Async XLA Ops:
  6.5 310.7 %copy-start = (bf16[1,704,2048]{2,1,0:T(8,128)(2,1)S(1)}, bf16[1,704,2048]{2,1,0:T(8,128)(2,1)}, u32[]{:S(2)}) copy-start(bf16[1,704,2048]{2,1,0:T(8,128)(2,1)} %param.35) | copy-start | bytes 8650756
  6.5 5.5 %copy-start.9 = (f32[256,4]{0,1:T(4,128)S(1)}, f32[256,4]{0,1:T(4,128)}, u32[]{:S(2)}) copy-start(f32[256,4]{0,1:T(4,128)} %param.27) | copy-start | bytes 12292
  6.5 172.3 %all-gather.14.cloned.1.call-start = ((), (), s32[]{:S(2)}) async-start(), calls=%async_computation.9 | async-start | bytes 9437184 | tf_op jit(solution)/shard_map/all_gather | solution.py:20
  12.0 7.8 %copy-start.6 = (bf16[256,1024]{1,0:T(8,128)(2,1)S(1)}, bf16[256,1024]{1,0:T(8,128)(2,1)}, u32[]{:S(2)}) copy-start(bf16[256,1024]{1,0:T(8,128)(2,1)} %param.22) | copy-start | bytes 1572868
  21.3 2.7 copy-start.7
  48.6 2.8 copy-start.12
  51.3 196.8 %reduce-scatter.3.cloned.1.call-start = ((), (), s32[]{:S(2)}) async-start(), calls=%async_computation.4 | async-start | bytes 1310720 | tf_op jit(solution)/shard_map/reduce_scatter | solution.py:152
  206.5 4.5 %copy-start.1 = (bf16[2,128,4,512]{3,2,1,0:T(4,128)(2,1)S(1)}, bf16[2,128,4,512]{3,2,1,0:T(4,128)(2,1)}, u32[]{:S(2)}) copy-start(bf16[2,128,4,512]{3,2,1,0:T(4,128)(2,1)} %reshape_reshape.16) | copy-start | bytes 3145732
  206.5 4.5 %copy-start.5 = (f32[2,4,128,512]{3,2,0,1:T(8,128)S(1)}, f32[2,4,128,512]{3,2,0,1:T(8,128)}, u32[]{:S(2)}) copy-start(f32[2,4,128,512]{3,2,0,1:T(8,128)} %get-tuple-element.132) | copy-start | bytes 6291460
  214.4 1.6 copy-start.2
  218.2 29.9 %copy-start.3 = (bf16[64,2048]{1,0:T(8,128)(2,1)S(1)}, bf16[64,2048]{1,0:T(8,128)(2,1)}, u32[]{:S(2)}) copy-start(bf16[64,2048]{1,0:T(8,128)(2,1)} %param.20) | copy-start | bytes 786436
  218.2 31.1 %copy-start.8 = (f32[2048]{0:T(1024)S(1)}, f32[2048]{0:T(1024)}, u32[]{:S(2)}) copy-start(f32[2048]{0:T(1024)} %param.30) | copy-start | bytes 24580
  225.0 26.4 %copy-start.10 = (s32[256,2]{0,1:T(2,128)S(1)}, s32[256,2]{0,1:T(2,128)}, u32[]{:S(2)}) copy-start(s32[256,2]{0,1:T(2,128)} %param.31) | copy-start | bytes 6148
  225.0 42.9 %all-gather.8.cloned.1.call-start = ((), (), s32[]{:S(2)}) async-start(), calls=%async_computation.5 | async-start | bytes 1310720 | tf_op jit(solution)/shard_map/all_gather | solution.py:160
  251.1 60.9 %all-gather.10.cloned.1.call-start = ((), (), s32[]{:S(2)}) async-start(), calls=%async_computation.6 | async-start | bytes 2621440 | tf_op jit(solution)/shard_map/all_gather | solution.py:188
  291.1 65.0 %reduce-scatter.5.cloned.1.call-start = ((), (), s32[]{:S(2)}) async-start(), calls=%async_computation.7 | async-start | bytes 2621440 | tf_op jit(solution)/shard_map/reduce_scatter | solution.py:193
  324.8 78.0 %all-gather.12.cloned.1.call-start = ((), (), s32[]{:S(2)}) async-start(), calls=%async_computation.8 | async-start | bytes 2621440 | tf_op jit(solution)/shard_map/all_gather | solution.py:203
  386.1 13.2 %copy-start.11 = (f32[256,2]{0,1:T(2,128)S(1)}, f32[256,2]{0,1:T(2,128)}, u32[]{:S(2)}) copy-start(f32[256,2]{0,1:T(2,128)} %param.32) | copy-start | bytes 6148
  386.1 16.7 %copy-start.4 = (bf16[64,2048]{1,0:T(8,128)(2,1)S(1)}, bf16[64,2048]{1,0:T(8,128)(2,1)}, u32[]{:S(2)}) copy-start(bf16[64,2048]{1,0:T(8,128)(2,1)} %reduce-scatter.3.cloned.1.call-done) | copy-start | bytes 786436
Sparse Core Ops, SparseCore 0:
  51.4 127.3 all-gather.13
  225.1 22.9 reduce-scatter.2
  251.2 16.6 all-gather.7
  291.2 20.6 all-gather.9
  324.9 31.1 reduce-scatter.4
  378.4 20.6 all-gather.11
where the time goes:
time: 414 us; the launch traced here: 413 us
  waiting for transfers between devices  174 us (42%)
  blocking collectives  68.7 us (17%)
  other arithmetic  68.2 us (16%)
  matrix products  51.8 us (13%)
  local copies, waits for them, and re-layouts  36 us (9%)
  between operations  13.8 us (3%)
    all_gather x1, waiting for transfers between devices, entering(): lax.all_gather(part.astype(kind), axis)  94.6 us
    reduce_scatter x1, waiting for transfers between devices, body(): lax.psum_scatter(jnp.dot(hidden, expert_down[0], preferred_element_type=j...  31.3 us
    all_gather x1, blocking collectives, entering(): lax.all_gather(part.astype(kind), axis)  28.9 us
    select_n x8, other arithmetic, step(): return jax.tree.map(lambda a, b: jnp.where(reached, a, b), new, before)  27.7 us
    reduce_scatter x1, waiting for transfers between devices, body(): lax.psum_scatter(jnp.dot(mixed, output_matrix, preferred_element_type=jnp...  23.1 us
    all_gather x1, waiting for transfers between devices, body(): arrived = lax.all_gather(shared, 'tp', axis=0, tiled=True)  20.8 us
    all_to_all x1, blocking collectives, body(): lax.all_to_all(filled.astype(jnp.bfloat16).reshape(block_slots, experts,...  20.2 us
    all_to_all x1, blocking collectives, body(): lax.all_to_all(expert_token_rows, 'sp', split_axis=1, concat_axis=1, tile...  19.7 us
  transfers between devices with their start and end apart: 6, of which 5 were waited for; matrix products, arithmetic and copies ran while one was open for 10% of the time, Pallas kernels for 0%

commit v1 on v0

v1 whole, which is shorter than its diff:
```python
import functools

import jax
import jax.numpy as jnp
from jax import lax
from jax.experimental import pallas as pl
from jax.experimental.pallas import tpu as pltpu
from jax.sharding import PartitionSpec as P

HK = 256
HV = 512
TOP = 2
BLK = 128
TEMPER = 16.0
EPSILON = 1e-06
HIGHEST = lax.Precision.HIGHEST
MESH = pl.DeviceIdType.MESH
F32 = jnp.float32
BF16 = jnp.bfloat16


def mm(a, b, ca, cb, precision=None):
    return lax.dot_general(
        a, b, (((ca,), (cb,)), ((), ())), preferred_element_type=F32, precision=precision
    )


def remote(src, dst, send, recv, target):
    return pltpu.make_async_remote_copy(
        src_ref=src, dst_ref=dst, send_sem=send, recv_sem=recv, device_id=target, device_id_type=MESH
    )


def scatter_sum(src, r1, half, r2, s1, q1, s2, q2, y, c, ny, sent):
    partner = {"tp": 2 * y + 1 - c}
    for i in range(1, ny + 1):
        to = lax.rem(y + i, ny)
        copy = remote(src.at[to, 1 - c], r1.at[to], s1.at[to], q1.at[to], partner)
        copy.start()
        sent.append(copy)
    for i in range(1, ny):
        to = lax.rem(y + i, ny)
        remote(src.at[to, c], r1.at[to], s1.at[to], q1.at[to], partner).wait_recv()
        half[to] = (src[to, c].astype(F32) + r1[to].astype(F32)).astype(BF16)
        copy = remote(half.at[to], r2.at[y], s2.at[to], q2.at[y], {"tp": 2 * to + c})
        copy.start()
        sent.append(copy)
    remote(src.at[y, c], r1.at[y], s1.at[y], q1.at[y], partner).wait_recv()
    total = src[y, c].astype(F32) + r1[y].astype(F32)
    for i in range(1, ny):
        to = lax.rem(y + i, ny)
        remote(half.at[to], r2.at[to], s2.at[to], q2.at[to], {"tp": 2 * to + c}).wait_recv()
        total = total + r2[to].astype(F32)
    return total


def layer_kernel(
    n, nt, hs,
    stream, q, k, v, low, mat, bias, shift, gain, wout, fgain, routes, rweights, wgate, wup, wdown,
    out,
    ins, prior, sbuf, rbuf, cbuf, carry, dec, decall, acc, qs,
    wo, wg, wu, wd, mixed,
    prod, p1, ph, p2, mid, group, selt, wcomb, fb, rows, pb, r4, hb, r5, part, t1, th, t2,
    wsem, sa, ra, sd, rd, sb, rb, sp1, rp1, sp2, rp2, sg, rg, sgc, rgc, sx, rx, sxc, rxc,
    s4, q4, s5, q5, st1, rt1, st2, rt2,
):
    me = lax.axis_index("sp")
    t = lax.axis_index("tp")
    y = t // 2
    c = lax.rem(t, 2)
    ny = nt // 2
    partner = {"tp": 2 * y + 1 - c}
    length = q.shape[0]
    heads = q.shape[1] // HK
    blocks = length // BLK
    width = stream.shape[1]
    rows_here = stream.shape[0]
    sent = []

    barrier = pltpu.get_barrier_semaphore()
    for i in range(1, n):
        pl.semaphore_signal(barrier, inc=1, device_id={"sp": lax.rem(me + i, n)}, device_id_type=MESH)
    for i in range(1, ny):
        pl.semaphore_signal(
            barrier, inc=1, device_id={"tp": 2 * lax.rem(y + i, ny) + c}, device_id_type=MESH
        )
    pl.semaphore_signal(barrier, inc=1, device_id=partner, device_id_type=MESH)

    loads = [
        pltpu.make_async_copy(wout, wo, wsem.at[0]),
        pltpu.make_async_copy(wgate.at[0], wg, wsem.at[1]),
        pltpu.make_async_copy(wup.at[0], wu, wsem.at[2]),
        pltpu.make_async_copy(wdown.at[0], wd, wsem.at[3]),
    ]
    for load in loads:
        load.start()

    row_id = lax.broadcasted_iota(jnp.int32, (BLK, BLK), 0)
    col_id = lax.broadcasted_iota(jnp.int32, (BLK, BLK), 1)
    causal = row_id >= col_id
    tril = causal.astype(F32)

    for h in range(heads):
        ks, vs = slice(h * HK, (h + 1) * HK), slice(h * HV, (h + 1) * HV)
        pre = mm(low[...], mat[:, ks], 1, 0) + bias[:, ks]
        logged = (jnp.minimum(pre, 0.0) - jnp.log1p(jnp.exp(-jnp.abs(pre)))) / TEMPER + shift[:, h : h + 1]
        state = None
        whole = None
        for b in range(blocks):
            at = slice(b * BLK, (b + 1) * BLK)
            inside = mm(tril, logged[at], 1, 0, HIGHEST)
            ins[at, ks] = inside
            last = inside[BLK - 1 : BLK, :]
            end = (k[at, ks].astype(F32) * jnp.exp(last - inside)).astype(BF16)
            added = mm(v[at, vs], end, 0, 0)
            state = added if state is None else state * jnp.exp(last) + added
            whole = last if whole is None else whole + last
            if b < blocks - 1:
                prior[b, :, ks] = state.astype(BF16)
        sbuf[:, :, ks] = state.astype(BF16).reshape(n, HV // n, HK)
        dec[:, ks] = jnp.exp(whole)

    pl.semaphore_wait(barrier, n - 1 + ny - 1 + 1)
    for i in range(1, n):
        to = lax.rem(me + i, n)
        copy = remote(dec, decall.at[me], sd.at[to], rd.at[me], {"sp": to})
        copy.start()
        sent.append(copy)
        copy = remote(sbuf.at[to], rbuf.at[me], sa.at[to], ra.at[me], {"sp": to})
        copy.start()
        sent.append(copy)
    rbuf[me] = sbuf[me]
    decall[me] = dec[...]

    for h in range(heads):
        ks, vs = slice(h * HK, (h + 1) * HK), slice(h * HV, (h + 1) * HV)
        passed = None
        for b in range(blocks):
            at = slice(b * BLK, (b + 1) * BLK)
            inside = ins[at, ks]
            last = inside[BLK - 1 : BLK, :]
            centre = last * 0.5
            qf = q[at, ks].astype(F32) * HK ** (-0.5)
            sq = (qf * jnp.exp(inside - centre)).astype(BF16)
            sk = (k[at, ks].astype(F32) * jnp.exp(centre - inside)).astype(BF16)
            scores = jnp.where(causal, mm(sq, sk, 1, 1), 0.0).astype(BF16)
            local = mm(scores, v[at, vs], 1, 0)
            full = inside if passed is None else inside + passed
            qs[at, ks] = (qf * jnp.exp(full)).astype(BF16)
            if b > 0:
                local = local + mm((qf * jnp.exp(inside)).astype(BF16), prior[b - 1, :, ks], 1, 1)
            passed = last if passed is None else passed + last
            acc[at, vs] = local

    total = jnp.zeros((HV // n, heads * HK), F32)
    for j in range(n):
        cbuf[j] = total.astype(BF16)

        @pl.when(j != me)
        def _():
            remote(cbuf.at[j], carry.at[me], sb.at[j], rb.at[me], {"sp": j}).start()
            remote(dec, decall.at[j], sd.at[j], rd.at[j], {"sp": j}).wait_recv()
            remote(sbuf.at[j], rbuf.at[j], sa.at[j], ra.at[j], {"sp": j}).wait_recv()

        total = total * decall[j] + rbuf[j].astype(F32)
    carry[me] = cbuf[me]

    lane = lax.broadcasted_iota(jnp.int32, (length, n), 1)
    first = (routes[:, 0:1] == lane).astype(F32)
    second = (routes[:, 1:2] == lane).astype(F32)
    earlier = (
        lax.broadcasted_iota(jnp.int32, (length, length), 0)
        > lax.broadcasted_iota(jnp.int32, (length, length), 1)
    ).astype(BF16)
    counts = mm(earlier, (first + second).astype(BF16), 1, 0)
    slot_lane = lax.broadcasted_iota(jnp.int32, (length, n * hs), 1).astype(F32)
    base = (c * hs).astype(F32)
    chosen = jnp.zeros((length, n * hs), F32)
    weighted = jnp.zeros((length, n * hs), F32)
    for j, mask in enumerate((first, second)):
        rank = jnp.sum(counts * mask, axis=1, keepdims=True) - base
        place = jnp.where(
            (rank >= 0) & (rank < hs), routes[:, j : j + 1].astype(F32) * hs + rank, -1.0
        )
        hit = place == slot_lane
        chosen = chosen + jnp.where(hit, 1.0, 0.0)
        weighted = weighted + jnp.where(hit, rweights[:, j : j + 1], 0.0)
    selt[...] = chosen.astype(BF16)
    wcomb[...] = weighted.astype(BF16)

    for i in range(1, n):
        j = lax.rem(me + i, n)
        remote(cbuf.at[j], carry.at[j], sb.at[j], rb.at[j], {"sp": j}).wait()
    for h in range(heads):
        ks, vs = slice(h * HK, (h + 1) * HK), slice(h * HV, (h + 1) * HV)
        x = acc[:, vs] + mm(qs[:, ks], carry[:, :, ks].reshape(HV, HK), 1, 1)
        scale = lax.rsqrt(jnp.mean(x * x, axis=-1, keepdims=True) + EPSILON)
        mixed[:, vs] = (x * scale * gain[...]).astype(BF16)

    loads[0].wait()
    tile = 256

    @pl.loop(0, width // tile)
    def _(i):
        at = pl.ds(pl.multiple_of(i * tile, tile), tile)
        piece = mm(mixed[...], wo[:, at], 1, 0).astype(BF16)
        prod[:, :, :, at] = piece.reshape(ny, 2, rows_here, tile)

    attended = scatter_sum(prod, p1, ph, p2, sp1, rp1, sp2, rp2, y, c, ny, sent)
    midstream = stream[...].astype(F32) + attended
    mid[...] = midstream
    scale = lax.rsqrt(jnp.mean(midstream * midstream, axis=-1, keepdims=True) + EPSILON)
    group[y, c] = (midstream * scale * fgain[...]).astype(BF16)

    for i in range(1, ny):
        to = lax.rem(y + i, ny)
        copy = remote(group.at[y, c], group.at[y, c], sg.at[to], rg.at[y], {"tp": 2 * to + c})
        copy.start()
        sent.append(copy)
    copy = remote(group.at[y, c], group.at[y, c], sgc.at[y], rgc.at[y], partner)
    copy.start()
    sent.append(copy)
    for i in range(1, ny):
        to = lax.rem(y + i, ny)
        remote(group.at[to, c], group.at[to, c], sg.at[to], rg.at[to], {"tp": 2 * to + c}).wait_recv()
        copy = remote(group.at[to, c], group.at[to, c], sgc.at[to], rgc.at[to], partner)
        copy.start()
        sent.append(copy)
    for i in range(ny):
        to = lax.rem(y + i, ny)
        remote(group.at[to, 1 - c], group.at[to, 1 - c], sgc.at[to], rgc.at[to], partner).wait_recv()

    @pl.loop(0, width // tile)
    def _(i):
        at = pl.ds(pl.multiple_of(i * tile, tile), tile)
        picked = mm(selt[...], group[:, :, :, at].reshape(length, tile), 0, 0)
        fb[:, :, at] = picked.astype(BF16).reshape(n, hs, tile)

    for i in range(1, n):
        to = lax.rem(me + i, n)
        copy = remote(fb.at[to], rows.at[me, c], sx.at[to], rx.at[me], {"sp": to})
        copy.start()
        sent.append(copy)
    copy = remote(fb.at[me], rows.at[me, c], sxc.at[me], rxc.at[me], partner)
    copy.start()
    sent.append(copy)
    rows[me, c] = fb[me]
    for i in range(1, n):
        j = lax.rem(me + n - i, n)
        remote(fb.at[j], rows.at[j, c], sx.at[j], rx.at[j], {"sp": j}).wait_recv()
        copy = remote(rows.at[j, c], rows.at[j, c], sxc.at[j], rxc.at[j], partner)
        copy.start()
        sent.append(copy)
    for i in range(n):
        j = lax.rem(me + n - i, n)
        remote(rows.at[j, 1 - c], rows.at[j, 1 - c], sxc.at[j], rxc.at[j], partner).wait_recv()

    for load in loads[1:]:
        load.wait()
    step = max(1, min(n, 256 // (2 * hs)))

    @pl.loop(0, n // step)
    def _(g):
        here = pl.ds(g * step, step)
        taken = rows[here].reshape(step * 2 * hs, width)
        gated = mm(taken, wg[...], 1, 0)
        lifted = mm(taken, wu[...], 1, 0)
        hidden = (gated * jax.nn.sigmoid(gated) * lifted).astype(BF16)

        @pl.loop(0, width // 512)
        def _(i):
            at = pl.ds(pl.multiple_of(i * 512, 512), 512)
            piece = mm(hidden, wd[:, at], 1, 0).astype(BF16)
            pb[here, :, :, at] = piece.reshape(step, 2, hs, 512)

    for i in range(1, n + 1):
        j = lax.rem(me + i, n)
        copy = remote(pb.at[j, 1 - c], r4.at[j], s4.at[j], q4.at[j], partner)
        copy.start()
        sent.append(copy)
    for i in range(1, n + 1):
        j = lax.rem(me + i, n)
        remote(pb.at[j, c], r4.at[j], s4.at[j], q4.at[j], partner).wait_recv()
        both = (pb[j, c].astype(F32) + r4[j].astype(F32)).astype(BF16)
        if i == n:
            r5[me] = both
        else:
            hb[j] = both
            copy = remote(hb.at[j], r5.at[me], s5.at[j], q5.at[me], {"sp": j})
            copy.start()
            sent.append(copy)
    for i in range(1, n):
        j = lax.rem(me + n - i, n)
        remote(hb.at[j], r5.at[j], s5.at[j], q5.at[j], {"sp": j}).wait_recv()

    @pl.loop(0, width // tile)
    def _(i):
        at = pl.ds(pl.multiple_of(i * tile, tile), tile)
        piece = mm(wcomb[...], r5[:, :, at].reshape(n * hs, tile), 1, 0).astype(BF16)
        part[:, :, :, at] = piece.reshape(ny, 2, rows_here, tile)

    routed = scatter_sum(part, t1, th, t2, st1, rt1, st2, rt2, y, c, ny, sent)
    out[...] = (mid[...] + routed).astype(BF16)
    for copy in sent:
        copy.wait_send()


def solution(mesh):
    n, nt = mesh.shape["sp"], mesh.shape["tp"]
    ny = nt // 2

    def body(
        stream_in, queries, key_rows, values, decay_low, decay_matrix, decay_bias, decay_shift,
        head_gain, output_matrix, feed_gain, routes, route_weights, expert_gate, specialist_widen,
        expert_down,
    ):
        length, keys = queries.shape
        vals = values.shape[1]
        rows_here, width = stream_in.shape
        hidden = expert_gate.shape[2]
        capacity = nt * max(1, TOP * length // (n * nt))
        hs = capacity // 2
        blocks = length // BLK
        vm = pltpu.VMEM
        dma = pltpu.SemaphoreType.DMA
        scratch = [
            vm((length, keys), F32), vm((max(1, blocks - 1), HV, keys), BF16),
            vm((n, HV // n, keys), BF16), vm((n, HV // n, keys), BF16),
            vm((n, HV // n, keys), BF16), vm((n, HV // n, keys), BF16),
            vm((1, keys), F32), vm((n, 1, keys), F32),
            vm((length, vals), F32), vm((length, keys), BF16),
            vm(output_matrix.shape, BF16), vm((width, hidden), BF16), vm((width, hidden), BF16),
            vm((hidden, width), BF16), vm((length, vals), BF16),
            vm((ny, 2, rows_here, width), BF16), vm((ny, rows_here, width), BF16),
            vm((ny, rows_here, width), BF16), vm((ny, rows_here, width), BF16),
            vm((rows_here, width), F32), vm((ny, 2, rows_here, width), BF16),
            vm((length, n * hs), BF16), vm((length, n * hs), BF16),
            vm((n, hs, width), BF16), vm((n, 2, hs, width), BF16), vm((n, 2, hs, width), BF16),
            vm((n, hs, width), BF16), vm((n, hs, width), BF16), vm((n, hs, width), BF16),
            vm((ny, 2, rows_here, width), BF16), vm((ny, rows_here, width), BF16),
            vm((ny, rows_here, width), BF16), vm((ny, rows_here, width), BF16),
            dma((4,)),
            dma((n,)), dma((n,)), dma((n,)), dma((n,)), dma((n,)), dma((n,)),
            dma((ny,)), dma((ny,)), dma((ny,)), dma((ny,)),
            dma((ny,)), dma((ny,)), dma((ny,)), dma((ny,)),
            dma((n,)), dma((n,)), dma((n,)), dma((n,)),
            dma((n,)), dma((n,)), dma((n,)), dma((n,)),
            dma((ny,)), dma((ny,)), dma((ny,)), dma((ny,)),
        ]
        near = pl.BlockSpec(memory_space=pltpu.VMEM)
        far = pl.BlockSpec(memory_space=pl.ANY)
        return pl.pallas_call(
            functools.partial(layer_kernel, n, nt, hs),
            out_shape=jax.ShapeDtypeStruct((rows_here, width), BF16),
            in_specs=[near] * 9 + [far] + [near] * 3 + [far] * 3,
            out_specs=near,
            scratch_shapes=scratch,
            compiler_params=pltpu.CompilerParams(
                collective_id=0, has_side_effects=True, vmem_limit_bytes=64_000_000
            ),
            name="layer",
        )(
            stream_in, queries, key_rows, values, decay_low, decay_matrix, decay_bias.reshape(1, -1),
            decay_shift, head_gain.reshape(1, -1), output_matrix, feed_gain.reshape(1, -1), routes,
            route_weights, expert_gate, specialist_widen, expert_down,
        )

    return jax.shard_map(
        body,
        mesh=mesh,
        in_specs=(
            P(("sp", "tp"), None), P("sp", "tp"), P("sp", "tp"), P("sp", "tp"), P("sp", None),
            P(None, "tp"), P("tp"), P("sp", "tp"), P(), P("tp", None), P(), P("sp", None),
            P("sp", None), P("sp", None, "tp"), P("sp", None, "tp"), P("sp", "tp", None),
        ),
        out_specs=P(("sp", "tp"), None),
        check_vma=False,
    )
```

time: 414 us -> 163 us (0.39)
  the two profiles are of different devices: /device:TPU:0 before, /device:TPU:27 now
where the time goes in v1:
time: 163 us
  Pallas kernels  147 us (90%)
  local copies, waits for them, and re-layouts  15.1 us (9%)
    pallas_call x1, Pallas kernels, body(): pl.pallas_call(functools.partial(layer_kernel, n, nt, hs), out_shape=jax....  147 us
    unnamed x9, local copies, waits for them, and re-layouts  15.1 us

profile of v1, /device:TPU:27, one launch (start us, length us, event | category | flops | bytes accessed | tf_op | source)
XLA Modules:
  0.0 162.6 jit_solution(2665506600785607191)
XLA Ops:
  0.0 1.4 copy.17.low
  1.4 1.5 copy.18.shift
  2.9 0.0 copy-start
  2.9 1.6 copy.19.routes
  4.5 1.5 copy.20.rweights
  6.0 4.6 %copy.21.wgate = bf16[1,2048,704]{2,1,0:T(8,128)(2,1)} copy(bf16[1,2048,704]{1,2,0:T(8,128)(2,1)} %param.29) | data formatting | bytes 5767168 | tf_op args[13]
  10.6 0.0 copy-done
  10.6 2.8 %copy.22.wup = bf16[1,2048,704]{2,1,0:T(8,128)(2,1)} copy(bf16[1,2048,704]{1,2,0:T(8,128)(2,1)S(1)} %copy-done) | data formatting | bytes 5767168 | tf_op args[14]
  13.4 147.5 %layer.1 = bf16[64,2048]{1,0:T(8,128)(2,1)} custom-call(bf16[64,2048]{1,0:T(8,128)(2,1)} %stream.1, bf16[256,1024]{1,0:T(8,128)(2,1)} %q.1, bf16[256,1024]{1,0:T(8,128)(2,1)} %k.1, bf16[256,2048]{1,0:T(8,128)(2,1)} %v.1, bf16[256,16]{1,0:T(8,128)(2,1)} %copy.17.low, bf16[16,1024]{1,0:T(8,128)(2,1)} %mat.1, f32[1,1024]{1,0:T(1,128)} %bitcast.4, ...), custom_call_target="tpu_custom_call" | custom-call | tf_op jit(solution)/shard_map/layer/pallas_call | solution.py:352
  160.9 1.7 %copy.24 = bf16[64,2048]{1,0:T(8,128)(2,1)} copy(bf16[64,2048]{1,0:T(8,128)(2,1)} %layer.1) | data formatting | bytes 524288
Async XLA Ops:
  2.9 7.7 %copy-start = (bf16[1,2048,704]{1,2,0:T(8,128)(2,1)S(1)}, bf16[1,2048,704]{1,2,0:T(8,128)(2,1)}, u32[]{:S(2)}) copy-start(bf16[1,2048,704]{1,2,0:T(8,128)(2,1)} %param.30) | copy-start | bytes 8650756

commit v2 on v1

--- a/solution.py
+++ b/solution.py
@@ -55,20 +55,24 @@
 
 
 def layer_kernel(
-    n, nt, hs,
+    n, nt, hs, size, yl,
     stream, q, k, v, low, mat, bias, shift, gain, wout, fgain, routes, rweights, wgate, wup, wdown,
     out,
-    ins, prior, sbuf, rbuf, cbuf, carry, dec, decall, acc, qs,
+    ins, prior, sbuf, rbuf, cbuf, carry, tsend, trecv, dec, decall, acc, qs,
     wo, wg, wu, wd, mixed,
-    prod, p1, ph, p2, mid, group, selt, wcomb, fb, rows, pb, r4, hb, r5, part, t1, th, t2,
-    wsem, sa, ra, sd, rd, sb, rb, sp1, rp1, sp2, rp2, sg, rg, sgc, rgc, sx, rx, sxc, rxc,
-    s4, q4, s5, q5, st1, rt1, st2, rt2,
+    prod, p1, ph, p2, mid, group, selt, wcomb, fb, rows, pb, r4, hy, r6, hb, r5, part, t1, th, t2,
+    wsem, sa, ra, sd, rd, sb, rb, stt, rtt, sp1, rp1, sp2, rp2, sg, rg, sgc, rgc, sx, rx, sy, ry, sxc, rxc,
+    s4, q4, s6, q6, s5, q5, st1, rt1, st2, rt2,
 ):
     me = lax.axis_index("sp")
     t = lax.axis_index("tp")
     y = t // 2
     c = lax.rem(t, 2)
     ny = nt // 2
+    mine, team, teams = lax.rem(me, size), me // size, n // size
+    first_one = team * size
+    yo = y if yl > 1 else 0
+    part_of = 2 * yo + c
     partner = {"tp": 2 * y + 1 - c}
     length = q.shape[0]
     heads = q.shape[1] // HK
@@ -100,40 +104,87 @@
     causal = row_id >= col_id
     tril = causal.astype(F32)
 
+    shifts = shift[...].T
+
     for h in range(heads):
-        ks, vs = slice(h * HK, (h + 1) * HK), slice(h * HV, (h + 1) * HV)
-        pre = mm(low[...], mat[:, ks], 1, 0) + bias[:, ks]
-        logged = (jnp.minimum(pre, 0.0) - jnp.log1p(jnp.exp(-jnp.abs(pre)))) / TEMPER + shift[:, h : h + 1]
-        state = None
+        ks = slice(h * HK, (h + 1) * HK)
+        pre = mm(low[...], mat[:, ks], 0, 0) + bias[:, ks]
+        logged = (jnp.minimum(pre, 0.0) - jnp.log1p(jnp.exp(-jnp.abs(pre)))) / TEMPER + shifts[:, h : h + 1]
         whole = None
         for b in range(blocks):
             at = slice(b * BLK, (b + 1) * BLK)
             inside = mm(tril, logged[at], 1, 0, HIGHEST)
             ins[at, ks] = inside
             last = inside[BLK - 1 : BLK, :]
+            whole = last if whole is None else whole + last
+        dec[:, ks] = jnp.exp(whole)
+    decall[mine] = dec[...]
+
+    for h in range(heads):
+        ks, vs = slice(h * HK, (h + 1) * HK), slice(h * HV, (h + 1) * HV)
+        state = None
+        for b in range(blocks):
+            at = slice(b * BLK, (b + 1) * BLK)
+            inside = ins[at, ks]
+            last = inside[BLK - 1 : BLK, :]
             end = (k[at, ks].astype(F32) * jnp.exp(last - inside)).astype(BF16)
             added = mm(v[at, vs], end, 0, 0)
             state = added if state is None else state * jnp.exp(last) + added
-            whole = last if whole is None else whole + last
             if b < blocks - 1:
                 prior[b, :, ks] = state.astype(BF16)
-        sbuf[:, :, ks] = state.astype(BF16).reshape(n, HV // n, HK)
-        dec[:, ks] = jnp.exp(whole)
-
-    pl.semaphore_wait(barrier, n - 1 + ny - 1 + 1)
-    for i in range(1, n):
-        to = lax.rem(me + i, n)
-        copy = remote(dec, decall.at[me], sd.at[to], rd.at[me], {"sp": to})
-        copy.start()
-        sent.append(copy)
-        copy = remote(sbuf.at[to], rbuf.at[me], sa.at[to], ra.at[me], {"sp": to})
-        copy.start()
-        sent.append(copy)
-    rbuf[me] = sbuf[me]
-    decall[me] = dec[...]
-
+        sbuf[h] = state.astype(BF16).reshape(size, HV // size, HK)
+        if h == 0:
+            pl.semaphore_wait(barrier, n - 1 + ny - 1 + 1)
+            for i in range(1, size):
+                to = lax.rem(mine + i, size)
+                copy = remote(dec, decall.at[mine], sd.at[to], rd.at[mine], {"sp": first_one + to})
+                copy.start()
+                sent.append(copy)
+        for i in range(1, size):
+            to = lax.rem(mine + i, size)
+            copy = remote(
+                sbuf.at[h, to], rbuf.at[h, mine], sa.at[h, to], ra.at[h, mine], {"sp": first_one + to}
+            )
+            copy.start()
+            sent.append(copy)
+        rbuf[h, mine] = sbuf[h, mine]
+
+    for i in range(1, size):
+        j = lax.rem(mine + i, size)
+        remote(dec, decall.at[j], sd.at[j], rd.at[j], {"sp": first_one + j}).wait_recv()
+    onward = {"sp": lax.rem(me + size, n)}
     for h in range(heads):
         ks, vs = slice(h * HK, (h + 1) * HK), slice(h * HV, (h + 1) * HV)
+        for i in range(1, size):
+            j = lax.rem(mine + i, size)
+            remote(sbuf.at[h, j], rbuf.at[h, j], sa.at[h, j], ra.at[h, j], {"sp": first_one + j}).wait_recv()
+        link = remote(tsend.at[h], trecv.at[h], stt.at[h], rtt.at[h], onward)
+
+        @pl.when(team > 0)
+        def _():
+            link.wait_recv()
+
+        @pl.when(team == 0)
+        def _():
+            trecv[h] = jnp.zeros_like(trecv[h])
+
+        total = trecv[h].astype(F32)
+        for j in range(size):
+            cbuf[h, j] = total.astype(BF16)
+            total = total * decall[j][:, ks] + rbuf[h, j].astype(F32)
+
+        @pl.when(team < teams - 1)
+        def _():
+            tsend[h] = total.astype(BF16)
+            link.start()
+
+        for i in range(1, size):
+            j = lax.rem(mine + i, size)
+            remote(
+                cbuf.at[h, j], carry.at[h, mine], sb.at[h, j], rb.at[h, mine], {"sp": first_one + j}
+            ).start()
+        carry[h, mine] = cbuf[h, mine]
+
         passed = None
         for b in range(blocks):
             at = slice(b * BLK, (b + 1) * BLK)
@@ -152,48 +203,37 @@
             passed = last if passed is None else passed + last
             acc[at, vs] = local
 
-    total = jnp.zeros((HV // n, heads * HK), F32)
-    for j in range(n):
-        cbuf[j] = total.astype(BF16)
-
-        @pl.when(j != me)
-        def _():
-            remote(cbuf.at[j], carry.at[me], sb.at[j], rb.at[me], {"sp": j}).start()
-            remote(dec, decall.at[j], sd.at[j], rd.at[j], {"sp": j}).wait_recv()
-            remote(sbuf.at[j], rbuf.at[j], sa.at[j], ra.at[j], {"sp": j}).wait_recv()
-
-        total = total * decall[j] + rbuf[j].astype(F32)
-    carry[me] = cbuf[me]
-
-    lane = lax.broadcasted_iota(jnp.int32, (length, n), 1)
-    first = (routes[:, 0:1] == lane).astype(F32)
-    second = (routes[:, 1:2] == lane).astype(F32)
+    lane = lax.broadcasted_iota(jnp.int32, (length, n), 1).astype(F32)
+    named = routes[...].astype(F32).T
+    shares = rweights[...].T
+    first = (named[:, 0:1] == lane).astype(F32)
+    second = (named[:, 1:2] == lane).astype(F32)
     earlier = (
         lax.broadcasted_iota(jnp.int32, (length, length), 0)
         > lax.broadcasted_iota(jnp.int32, (length, length), 1)
     ).astype(BF16)
     counts = mm(earlier, (first + second).astype(BF16), 1, 0)
     slot_lane = lax.broadcasted_iota(jnp.int32, (length, n * hs), 1).astype(F32)
-    base = (c * hs).astype(F32)
+    base = (part_of * hs).astype(F32)
     chosen = jnp.zeros((length, n * hs), F32)
     weighted = jnp.zeros((length, n * hs), F32)
     for j, mask in enumerate((first, second)):
         rank = jnp.sum(counts * mask, axis=1, keepdims=True) - base
         place = jnp.where(
-            (rank >= 0) & (rank < hs), routes[:, j : j + 1].astype(F32) * hs + rank, -1.0
+            (rank >= 0) & (rank < hs), named[:, j : j + 1] * hs + rank, -1.0
         )
         hit = place == slot_lane
         chosen = chosen + jnp.where(hit, 1.0, 0.0)
-        weighted = weighted + jnp.where(hit, rweights[:, j : j + 1], 0.0)
+        weighted = weighted + jnp.where(hit, shares[:, j : j + 1], 0.0)
     selt[...] = chosen.astype(BF16)
     wcomb[...] = weighted.astype(BF16)
 
-    for i in range(1, n):
-        j = lax.rem(me + i, n)
-        remote(cbuf.at[j], carry.at[j], sb.at[j], rb.at[j], {"sp": j}).wait()
     for h in range(heads):
         ks, vs = slice(h * HK, (h + 1) * HK), slice(h * HV, (h + 1) * HV)
-        x = acc[:, vs] + mm(qs[:, ks], carry[:, :, ks].reshape(HV, HK), 1, 1)
+        for i in range(1, size):
+            j = lax.rem(mine + i, size)
+            remote(cbuf.at[h, j], carry.at[h, j], sb.at[h, j], rb.at[h, j], {"sp": first_one + j}).wait()
+        x = acc[:, vs] + mm(qs[:, ks], carry[h].reshape(HV, HK), 1, 1)
         scale = lax.rsqrt(jnp.mean(x * x, axis=-1, keepdims=True) + EPSILON)
         mixed[:, vs] = (x * scale * gain[...]).astype(BF16)
 
@@ -236,62 +276,105 @@
         picked = mm(selt[...], group[:, :, :, at].reshape(length, tile), 0, 0)
         fb[:, :, at] = picked.astype(BF16).reshape(n, hs, tile)
 
+    def pass_on(i):
+        if i > 0:
+            remote(fb.at[me], rows.at[i, part_of], sx.at[i], rx.at[i], {"sp": me_at(i)}).wait_recv()
+        block = fb.at[me] if i == 0 else rows.at[i, part_of]
+        for d in range(1, yl):
+            copy = remote(
+                block, rows.at[i, part_of], sy.at[i, d], ry.at[i, d], {"tp": 2 * lax.rem(y + d, ny) + c}
+            )
+            copy.start()
+            sent.append(copy)
+        copy = remote(block, rows.at[i, part_of], sxc.at[i, yo], rxc.at[i, yo], partner)
+        copy.start()
+        sent.append(copy)
+
+    def pass_over(i):
+        for d in range(1, yl):
+            other = lax.rem(y + ny - d, ny)
+            block = rows.at[i, 2 * other + c]
+            remote(block, block, sy.at[i, d], ry.at[i, d], {"tp": 2 * other + c}).wait_recv()
+            copy = remote(block, block, sxc.at[i, other], rxc.at[i, other], partner)
+            copy.start()
+            sent.append(copy)
+
+    def me_at(i):
+        return lax.rem(me + i, n)
+
     for i in range(1, n):
         to = lax.rem(me + i, n)
-        copy = remote(fb.at[to], rows.at[me, c], sx.at[to], rx.at[me], {"sp": to})
-        copy.start()
-        sent.append(copy)
-    copy = remote(fb.at[me], rows.at[me, c], sxc.at[me], rxc.at[me], partner)
-    copy.start()
-    sent.append(copy)
-    rows[me, c] = fb[me]
+        copy = remote(fb.at[to], rows.at[i, part_of], sx.at[i], rx.at[i], {"sp": to})
+        copy.start()
+        sent.append(copy)
+    pass_on(0)
+    rows[0, part_of] = fb[me]
     for i in range(1, n):
-        j = lax.rem(me + n - i, n)
-        remote(fb.at[j], rows.at[j, c], sx.at[j], rx.at[j], {"sp": j}).wait_recv()
-        copy = remote(rows.at[j, c], rows.at[j, c], sxc.at[j], rxc.at[j], partner)
-        copy.start()
-        sent.append(copy)
+        pass_on(i)
+        pass_over(i - 1)
+    pass_over(n - 1)
     for i in range(n):
-        j = lax.rem(me + n - i, n)
-        remote(rows.at[j, 1 - c], rows.at[j, 1 - c], sxc.at[j], rxc.at[j], partner).wait_recv()
+        for d in range(yl):
+            block = rows.at[i, 2 * d + 1 - c]
+            remote(block, block, sxc.at[i, d], rxc.at[i, d], partner).wait_recv()
 
     for load in loads[1:]:
         load.wait()
-    step = max(1, min(n, 256 // (2 * hs)))
-
-    @pl.loop(0, n // step)
-    def _(g):
-        here = pl.ds(g * step, step)
-        taken = rows[here].reshape(step * 2 * hs, width)
-        gated = mm(taken, wg[...], 1, 0)
-        lifted = mm(taken, wu[...], 1, 0)
+    parts = 2 * yl
+    step = max(1, min(n, 256 // (parts * hs)))
+    for g in range(n // step):
+        taken = rows[g * step : (g + 1) * step].reshape(step * parts * hs, width)
+        gated = mm(taken, wg[...], 1, 1)
+        lifted = mm(taken, wu[...], 1, 1)
         hidden = (gated * jax.nn.sigmoid(gated) * lifted).astype(BF16)
 
         @pl.loop(0, width // 512)
         def _(i):
             at = pl.ds(pl.multiple_of(i * 512, 512), 512)
             piece = mm(hidden, wd[:, at], 1, 0).astype(BF16)
-            pb[here, :, :, at] = piece.reshape(step, 2, hs, 512)
-
-    for i in range(1, n + 1):
-        j = lax.rem(me + i, n)
-        copy = remote(pb.at[j, 1 - c], r4.at[j], s4.at[j], q4.at[j], partner)
-        copy.start()
-        sent.append(copy)
-    for i in range(1, n + 1):
-        j = lax.rem(me + i, n)
-        remote(pb.at[j, c], r4.at[j], s4.at[j], q4.at[j], partner).wait_recv()
-        both = (pb[j, c].astype(F32) + r4[j].astype(F32)).astype(BF16)
-        if i == n:
-            r5[me] = both
-        else:
-            hb[j] = both
-            copy = remote(hb.at[j], r5.at[me], s5.at[j], q5.at[me], {"sp": j})
+            pb[g * step : (g + 1) * step, :, :, :, at] = piece.reshape(step, yl, 2, hs, 512)
+
+        for i in range(g * step, (g + 1) * step):
+            for d in range(yl):
+                copy = remote(pb.at[i, d, 1 - c], r4.at[i, d], s4.at[i, d], q4.at[i, d], partner)
+                copy.start()
+                sent.append(copy)
+
+    def over_core(i):
+        for d in range(yl):
+            remote(pb.at[i, d, c], r4.at[i, d], s4.at[i, d], q4.at[i, d], partner).wait_recv()
+        for d in range(1, yl):
+            other = lax.rem(y + d, ny)
+            hy[i, other] = (pb[i, other, c].astype(F32) + r4[i, other].astype(F32)).astype(BF16)
+            copy = remote(hy.at[i, other], r6.at[i, d], s6.at[i, d], q6.at[i, d], {"tp": 2 * other + c})
             copy.start()
             sent.append(copy)
+
+    def over_y(i):
+        both = pb[i, yo, c].astype(F32) + r4[i, yo].astype(F32)
+        for d in range(1, yl):
+            other = lax.rem(y + ny - d, ny)
+            remote(hy.at[i, 0], r6.at[i, d], s6.at[i, d], q6.at[i, d], {"tp": 2 * other + c}).wait_recv()
+            both = both + r6[i, d].astype(F32)
+        if i == 0:
+            r5[me] = both.astype(BF16)
+        else:
+            j = lax.rem(me + n - i, n)
+            hb[i] = both.astype(BF16)
+            copy = remote(hb.at[i], r5.at[me], s5.at[j], q5.at[me], {"sp": j})
+            copy.start()
+            sent.append(copy)
+
+    lag = 2
+    order = list(range(1, n)) + [0]
+    for at_step in range(n + lag):
+        if at_step < n:
+            over_core(order[at_step])
+        if at_step >= lag:
+            over_y(order[at_step - lag])
     for i in range(1, n):
         j = lax.rem(me + n - i, n)
-        remote(hb.at[j], r5.at[j], s5.at[j], q5.at[j], {"sp": j}).wait_recv()
+        remote(hb.at[i], r5.at[j], s5.at[j], q5.at[j], {"sp": j}).wait_recv()
 
     @pl.loop(0, width // tile)
     def _(i):
@@ -303,6 +386,11 @@
     out[...] = (mid[...] + routed).astype(BF16)
     for copy in sent:
         copy.wait_send()
+
+    @pl.when(team < teams - 1)
+    def _():
+        for h in range(heads):
+            remote(tsend.at[h], trecv.at[h], stt.at[h], rtt.at[h], onward).wait_send()
 
 
 def solution(mesh):
@@ -319,38 +407,44 @@
         rows_here, width = stream_in.shape
         hidden = expert_gate.shape[2]
         capacity = nt * max(1, TOP * length // (n * nt))
-        hs = capacity // 2
+        yl = ny if capacity // nt >= 8 else 1
+        hs = capacity // (2 * yl)
+        size = next(x for x in (4, 2, 1) if n % x == 0)
+        heads = keys // HK
         blocks = length // BLK
         vm = pltpu.VMEM
         dma = pltpu.SemaphoreType.DMA
         scratch = [
             vm((length, keys), F32), vm((max(1, blocks - 1), HV, keys), BF16),
-            vm((n, HV // n, keys), BF16), vm((n, HV // n, keys), BF16),
-            vm((n, HV // n, keys), BF16), vm((n, HV // n, keys), BF16),
-            vm((1, keys), F32), vm((n, 1, keys), F32),
+            *[vm((heads, size, HV // size, HK), BF16)] * 4,
+            *[vm((heads, HV // size, HK), BF16)] * 2,
+            vm((1, keys), F32), vm((size, 1, keys), F32),
             vm((length, vals), F32), vm((length, keys), BF16),
-            vm(output_matrix.shape, BF16), vm((width, hidden), BF16), vm((width, hidden), BF16),
+            vm(output_matrix.shape, BF16), vm((hidden, width), BF16), vm((hidden, width), BF16),
             vm((hidden, width), BF16), vm((length, vals), BF16),
             vm((ny, 2, rows_here, width), BF16), vm((ny, rows_here, width), BF16),
             vm((ny, rows_here, width), BF16), vm((ny, rows_here, width), BF16),
             vm((rows_here, width), F32), vm((ny, 2, rows_here, width), BF16),
             vm((length, n * hs), BF16), vm((length, n * hs), BF16),
-            vm((n, hs, width), BF16), vm((n, 2, hs, width), BF16), vm((n, 2, hs, width), BF16),
-            vm((n, hs, width), BF16), vm((n, hs, width), BF16), vm((n, hs, width), BF16),
+            vm((n, hs, width), BF16), vm((n, 2 * yl, hs, width), BF16),
+            vm((n, yl, 2, hs, width), BF16), vm((n, yl, hs, width), BF16),
+            vm((n, yl, hs, width), BF16), vm((n, yl, hs, width), BF16),
+            vm((n, hs, width), BF16), vm((n, hs, width), BF16),
             vm((ny, 2, rows_here, width), BF16), vm((ny, rows_here, width), BF16),
             vm((ny, rows_here, width), BF16), vm((ny, rows_here, width), BF16),
             dma((4,)),
-            dma((n,)), dma((n,)), dma((n,)), dma((n,)), dma((n,)), dma((n,)),
+            dma((heads, size)), dma((heads, size)), dma((size,)), dma((size,)),
+            dma((heads, size)), dma((heads, size)), dma((heads,)), dma((heads,)),
             dma((ny,)), dma((ny,)), dma((ny,)), dma((ny,)),
             dma((ny,)), dma((ny,)), dma((ny,)), dma((ny,)),
-            dma((n,)), dma((n,)), dma((n,)), dma((n,)),
-            dma((n,)), dma((n,)), dma((n,)), dma((n,)),
+            dma((n,)), dma((n,)), *[dma((n, yl))] * 4,
+            *[dma((n, yl))] * 4, dma((n,)), dma((n,)),
             dma((ny,)), dma((ny,)), dma((ny,)), dma((ny,)),
         ]
         near = pl.BlockSpec(memory_space=pltpu.VMEM)
         far = pl.BlockSpec(memory_space=pl.ANY)
         return pl.pallas_call(
-            functools.partial(layer_kernel, n, nt, hs),
+            functools.partial(layer_kernel, n, nt, hs, size, yl),
             out_shape=jax.ShapeDtypeStruct((rows_here, width), BF16),
             in_specs=[near] * 9 + [far] + [near] * 3 + [far] * 3,
             out_specs=near,
@@ -360,9 +454,9 @@
             ),
             name="layer",
         )(
-            stream_in, queries, key_rows, values, decay_low, decay_matrix, decay_bias.reshape(1, -1),
-            decay_shift, head_gain.reshape(1, -1), output_matrix, feed_gain.reshape(1, -1), routes,
-            route_weights, expert_gate, specialist_widen, expert_down,
+            stream_in, queries, key_rows, values, decay_low.T, decay_matrix, decay_bias.reshape(1, -1),
+            decay_shift.T, head_gain.reshape(1, -1), output_matrix, feed_gain.reshape(1, -1), routes.T,
+            route_weights.T, expert_gate.swapaxes(1, 2), specialist_widen.swapaxes(1, 2), expert_down,
         )
 
     return jax.shard_map(

time: 163 us -> 125 us (0.77)
  the two profiles are of different devices: /device:TPU:27 before, /device:TPU:0 now
where the time goes in v2:
time: 125 us
  Pallas kernels  123 us (98%)
  local copies, waits for them, and re-layouts  1.67 us (1%)
    pallas_call x1, Pallas kernels, body(): pl.pallas_call(functools.partial(layer_kernel, n, nt, hs, size, yl), out_...  123 us

profile of v2, /device:TPU:0, one launch (start us, length us, event | category | flops | bytes accessed | tf_op | source)
XLA Modules:
  0.0 125.1 jit_solution(9666492188976750093)
XLA Ops:
  0.0 123.5 %layer.1 = bf16[64,2048]{1,0:T(8,128)(2,1)} custom-call(bf16[64,2048]{1,0:T(8,128)(2,1)} %stream.1, bf16[256,1024]{1,0:T(8,128)(2,1)} %q.1, bf16[256,1024]{1,0:T(8,128)(2,1)} %k.1, bf16[256,2048]{1,0:T(8,128)(2,1)} %v.1, bf16[16,256]{1,0:T(8,128)(2,1)} %bitcast.11, bf16[16,1024]{1,0:T(8,128)(2,1)} %mat.1, f32[1,1024]{1,0:T(1,128)} %bitcast.13, ...), custom_call_target="tpu_custom_call" | custom-call | tf_op jit(solution)/shard_map/layer/pallas_call | solution.py:446
  123.5 1.7 %copy.18 = bf16[64,2048]{1,0:T(8,128)(2,1)} copy(bf16[64,2048]{1,0:T(8,128)(2,1)} %layer.1) | data formatting | bytes 524288

commit v3 on v2

--- a/solution.py
+++ b/solution.py
@@ -31,27 +31,41 @@
     )
 
 
-def scatter_sum(src, r1, half, r2, s1, q1, s2, q2, y, c, ny, sent):
+def scatter_sum(fill, store, src, r1, half, r2, s1, q1, s2, q2, y, c, ny, sent):
     partner = {"tp": 2 * y + 1 - c}
-    for i in range(1, ny + 1):
-        to = lax.rem(y + i, ny)
-        copy = remote(src.at[to, 1 - c], r1.at[to], s1.at[to], q1.at[to], partner)
-        copy.start()
-        sent.append(copy)
-    for i in range(1, ny):
-        to = lax.rem(y + i, ny)
-        remote(src.at[to, c], r1.at[to], s1.at[to], q1.at[to], partner).wait_recv()
-        half[to] = (src[to, c].astype(F32) + r1[to].astype(F32)).astype(BF16)
-        copy = remote(half.at[to], r2.at[y], s2.at[to], q2.at[y], {"tp": 2 * to + c})
-        copy.start()
-        sent.append(copy)
-    remote(src.at[y, c], r1.at[y], s1.at[y], q1.at[y], partner).wait_recv()
-    total = src[y, c].astype(F32) + r1[y].astype(F32)
-    for i in range(1, ny):
-        to = lax.rem(y + i, ny)
-        remote(half.at[to], r2.at[to], s2.at[to], q2.at[to], {"tp": 2 * to + c}).wait_recv()
-        total = total + r2[to].astype(F32)
-    return total
+    width = src.shape[-1]
+    sides = [(f, slice(f * width // 2, (f + 1) * width // 2)) for f in range(2)]
+
+    def first(to, f, at):
+        return remote(src.at[to, 1 - c, :, at], r1.at[to, :, at], s1.at[f, to], q1.at[f, to], partner)
+
+    def second(to, slot, f, at):
+        return remote(
+            half.at[to, :, at], r2.at[slot, :, at], s2.at[f, to], q2.at[f, slot], {"tp": 2 * to + c}
+        )
+
+    for f, at in sides:
+        fill(f)
+        for i in range(1, ny + 1):
+            copy = first(lax.rem(y + i, ny), f, at)
+            copy.start()
+            sent.append(copy)
+    for f, at in sides:
+        for i in range(1, ny):
+            to = lax.rem(y + i, ny)
+            first(to, f, at).wait_recv()
+            half[to, :, at] = (src[to, c, :, at].astype(F32) + r1[to, :, at].astype(F32)).astype(BF16)
+            copy = second(to, y, f, at)
+            copy.start()
+            sent.append(copy)
+    for f, at in sides:
+        first(y, f, at).wait_recv()
+        total = src[y, c, :, at].astype(F32) + r1[y, :, at].astype(F32)
+        for i in range(1, ny):
+            to = lax.rem(y + i, ny)
+            second(to, to, f, at).wait_recv()
+            total = total + r2[to, :, at].astype(F32)
+        store(at, total)
 
 
 def layer_kernel(
@@ -240,15 +254,18 @@
     loads[0].wait()
     tile = 256
 
-    @pl.loop(0, width // tile)
-    def _(i):
-        at = pl.ds(pl.multiple_of(i * tile, tile), tile)
-        piece = mm(mixed[...], wo[:, at], 1, 0).astype(BF16)
-        prod[:, :, :, at] = piece.reshape(ny, 2, rows_here, tile)
-
-    attended = scatter_sum(prod, p1, ph, p2, sp1, rp1, sp2, rp2, y, c, ny, sent)
-    midstream = stream[...].astype(F32) + attended
-    mid[...] = midstream
+    def project(f):
+        @pl.loop(f * (width // tile // 2), (f + 1) * (width // tile // 2))
+        def _(i):
+            at = pl.ds(pl.multiple_of(i * tile, tile), tile)
+            piece = mm(mixed[...], wo[:, at], 1, 0).astype(BF16)
+            prod[:, :, :, at] = piece.reshape(ny, 2, rows_here, tile)
+
+    def add_stream(at, total):
+        mid[:, at] = stream[:, at].astype(F32) + total
+
+    scatter_sum(project, add_stream, prod, p1, ph, p2, sp1, rp1, sp2, rp2, y, c, ny, sent)
+    midstream = mid[...]
     scale = lax.rsqrt(jnp.mean(midstream * midstream, axis=-1, keepdims=True) + EPSILON)
     group[y, c] = (midstream * scale * fgain[...]).astype(BF16)
 
@@ -307,22 +324,14 @@
         copy = remote(fb.at[to], rows.at[i, part_of], sx.at[i], rx.at[i], {"sp": to})
         copy.start()
         sent.append(copy)
-    pass_on(0)
-    rows[0, part_of] = fb[me]
-    for i in range(1, n):
-        pass_on(i)
-        pass_over(i - 1)
-    pass_over(n - 1)
-    for i in range(n):
-        for d in range(yl):
-            block = rows.at[i, 2 * d + 1 - c]
-            remote(block, block, sxc.at[i, d], rxc.at[i, d], partner).wait_recv()
-
-    for load in loads[1:]:
-        load.wait()
     parts = 2 * yl
     step = max(1, min(n, 256 // (parts * hs)))
-    for g in range(n // step):
+
+    def experts(g):
+        for i in range(g * step, (g + 1) * step):
+            for d in range(yl):
+                block = rows.at[i, 2 * d + 1 - c]
+                remote(block, block, sxc.at[i, d], rxc.at[i, d], partner).wait_recv()
         taken = rows[g * step : (g + 1) * step].reshape(step * parts * hs, width)
         gated = mm(taken, wg[...], 1, 1)
         lifted = mm(taken, wu[...], 1, 1)
@@ -339,6 +348,20 @@
                 copy = remote(pb.at[i, d, 1 - c], r4.at[i, d], s4.at[i, d], q4.at[i, d], partner)
                 copy.start()
                 sent.append(copy)
+
+    pass_on(0)
+    rows[0, part_of] = fb[me]
+    early = min(step + 1, n - 1)
+    for load in loads[1:]:
+        load.wait()
+    for i in range(1, n):
+        pass_on(i)
+        pass_over(i - 1)
+        if i == early and step < n:
+            experts(0)
+    pass_over(n - 1)
+    for g in range(1 if step < n else 0, n // step):
+        experts(g)
 
     def over_core(i):
         for d in range(yl):
@@ -376,14 +399,17 @@
         j = lax.rem(me + n - i, n)
         remote(hb.at[i], r5.at[j], s5.at[j], q5.at[j], {"sp": j}).wait_recv()
 
-    @pl.loop(0, width // tile)
-    def _(i):
-        at = pl.ds(pl.multiple_of(i * tile, tile), tile)
-        piece = mm(wcomb[...], r5[:, :, at].reshape(n * hs, tile), 1, 0).astype(BF16)
-        part[:, :, :, at] = piece.reshape(ny, 2, rows_here, tile)
-
-    routed = scatter_sum(part, t1, th, t2, st1, rt1, st2, rt2, y, c, ny, sent)
-    out[...] = (mid[...] + routed).astype(BF16)
+    def combine(f):
+        @pl.loop(f * (width // tile // 2), (f + 1) * (width // tile // 2))
+        def _(i):
+            at = pl.ds(pl.multiple_of(i * tile, tile), tile)
+            piece = mm(wcomb[...], r5[:, :, at].reshape(n * hs, tile), 1, 0).astype(BF16)
+            part[:, :, :, at] = piece.reshape(ny, 2, rows_here, tile)
+
+    def add_routed(at, total):
+        out[:, at] = (mid[:, at] + total).astype(BF16)
+
+    scatter_sum(combine, add_routed, part, t1, th, t2, st1, rt1, st2, rt2, y, c, ny, sent)
     for copy in sent:
         copy.wait_send()
 
@@ -435,11 +461,10 @@
             dma((4,)),
             dma((heads, size)), dma((heads, size)), dma((size,)), dma((size,)),
             dma((heads, size)), dma((heads, size)), dma((heads,)), dma((heads,)),
-            dma((ny,)), dma((ny,)), dma((ny,)), dma((ny,)),
-            dma((ny,)), dma((ny,)), dma((ny,)), dma((ny,)),
+            *[dma((2, ny))] * 4, *[dma((ny,))] * 4,
             dma((n,)), dma((n,)), *[dma((n, yl))] * 4,
             *[dma((n, yl))] * 4, dma((n,)), dma((n,)),
-            dma((ny,)), dma((ny,)), dma((ny,)), dma((ny,)),
+            *[dma((2, ny))] * 4,
         ]
         near = pl.BlockSpec(memory_space=pltpu.VMEM)
         far = pl.BlockSpec(memory_space=pl.ANY)

time: 125 us -> 122 us (0.976)
  Pallas kernels: 123 us -> 121 us
    pallas_call x1, Pallas kernels: 123 us -> 121 us  [body(): pl.pallas_call(functools.partial(layer_kernel, n, nt, hs, size, yl), out_...]
where the time goes in v3:
time: 122 us
  Pallas kernels  121 us (99%)
  local copies, waits for them, and re-layouts  1.67 us (1%)
    pallas_call x1, Pallas kernels, body(): pl.pallas_call(functools.partial(layer_kernel, n, nt, hs, size, yl), out_...  121 us

profile of v3, /device:TPU:0, one launch (start us, length us, event | category | flops | bytes accessed | tf_op | source)
XLA Modules:
  0.0 122.3 jit_solution(10698872036524222683)
XLA Ops:
  0.0 120.6 %layer.1 = bf16[64,2048]{1,0:T(8,128)(2,1)} custom-call(bf16[64,2048]{1,0:T(8,128)(2,1)} %stream.1, bf16[256,1024]{1,0:T(8,128)(2,1)} %q.1, bf16[256,1024]{1,0:T(8,128)(2,1)} %k.1, bf16[256,2048]{1,0:T(8,128)(2,1)} %v.1, bf16[16,256]{1,0:T(8,128)(2,1)} %bitcast.11, bf16[16,1024]{1,0:T(8,128)(2,1)} %mat.1, f32[1,1024]{1,0:T(1,128)} %bitcast.13, ...), custom_call_target="tpu_custom_call" | custom-call | tf_op jit(solution)/shard_map/layer/pallas_call | solution.py:471
  120.6 1.7 %copy.18 = bf16[64,2048]{1,0:T(8,128)(2,1)} copy(bf16[64,2048]{1,0:T(8,128)(2,1)} %layer.1) | data formatting | bytes 524288
